TPU v7x, 256 devices: a whole 4x4x8 slice. The times are simulated.
256 devices in a mesh: ep: 32 (over z, x), tp: 8 (over y, core).
Axes of the slice: x: 4, y: 4, z: 8, core: 2. Of those that a mesh axis runs over, the one named last changes fastest.
Arguments:
- queries: bfloat16 [4096, 4096], P('ep', 'tp'), may hold values from -6 to 6
- key_rows: bfloat16 [4096, 4096], P('ep', 'tp'), may hold values from -6 to 6
- value_rows: bfloat16 [4096, 4096], P('ep', 'tp'), may hold values from -6 to 6
- key_shift: bfloat16 [4096, 64], P('ep', 'tp'), may hold values from -20 to 1
- out_weight: bfloat16 [4096, 4096], P('tp'), may hold values from -0.09375 to 0.09375
- routed_rows: bfloat16 [4096, 4096], P('ep'), may hold values from -6 to 6
- expert_ids: int32 [4096, 2], P('ep'), may hold values from 0 to 31, as said below
- route_weights: float32 [4096, 2], P(('ep', 'tp')), may hold values from 0.2 to 1
- gate_weight: bfloat16 [32, 4096, 1024], P('ep', None, 'tp'), may hold values from -0.09375 to 0.09375
- up_weight: bfloat16 [32, 4096, 1024], P('ep', None, 'tp'), may hold values from -0.09375 to 0.09375
- down_weight: bfloat16 [32, 1024, 4096], P('ep', 'tp'), may hold values from -0.1875 to 0.1875
Outputs:
- mixed_rows: bfloat16 [4096, 4096], P(('ep', 'tp'))
- routed_out: bfloat16 [4096, 4096], P(('ep', 'tp'))
Inputs may be any that keep to these rules, and one draw needn't show every extreme that they name: `expert_ids`: the two ids of a token differ and lie in one group of 8 consecutive experts. Within each aligned block of 16 tokens no expert is named more than 2 times.
All inputs are finite; a program needn't handle non-finite values.
Results may differ from a plain program's by a relative error of at most 0.015.
Values may be sent and summed in bfloat16 or wider, within the bound.
No kernel may reach another device: no remote copies, remote signals or barrier semaphores. Data moves between devices by JAX's collectives and lax.ppermute only.
A program may use at most 128 MiB of HBM per device.

v0:
```python
import jax
import jax.numpy as jnp
from jax import lax
from jax.sharding import PartitionSpec as P

HEAD = 64
KEY_BLOCK = 512


def sent_together(arrays, axis, dim, along):
    both = jnp.concatenate(arrays, axis=along)
    result, at, finished = (lax.all_gather(both, axis, axis=dim, tiled=True), 0, [])
    for a in arrays:
        finished.append(lax.slice_in_dim(result, at, at + a.shape[along], axis=along))
        at += a.shape[along]
    return tuple(finished)


def in_blocks(value, dim, peers):
    before, after = (value.shape[:dim], value.shape[dim + 1 :])
    return jnp.moveaxis(value.reshape(*before, peers, -1, *after), dim, 0)


def sent_and_summed(value, axis, dim):
    tiles = in_blocks(value, dim, lax.axis_size(axis))
    arrived = lax.all_to_all(tiles, axis, split_axis=0, concat_axis=0, tiled=True)
    return arrived.astype(jnp.float32).sum(axis=0)


def stick_attend(query_rows, key_all, value_all, shift_all, first_pos):
    row_count = query_rows.shape[0]
    head_count = query_rows.shape[1]
    head_depth = query_rows.shape[2]
    query_pos = first_pos + jnp.arange(row_count, dtype=jnp.int32)
    last_block = (first_pos + row_count - 1) // KEY_BLOCK
    score_scale = head_depth ** (-0.5)

    def sweep_block(step_index, state_pair):
        running, logsum = state_pair
        row_start = (last_block - step_index) * KEY_BLOCK
        key_tile_block = lax.dynamic_slice_in_dim(key_all, row_start, KEY_BLOCK, 0).reshape(
            KEY_BLOCK, head_count, head_depth
        )
        value_block = lax.dynamic_slice_in_dim(value_all, row_start, KEY_BLOCK, 0).reshape(
            KEY_BLOCK, head_count, head_depth
        )
        shift_block = lax.dynamic_slice_in_dim(shift_all, row_start, KEY_BLOCK, 0).astype(
            jnp.float32
        )
        scores = (
            jnp.einsum(
                "thd,shd->hts", query_rows, key_tile_block, preferred_element_type=jnp.float32
            )
            * score_scale
        )
        scores = scores + shift_block.T[:, None, :]
        key_pos = row_start + jnp.arange(KEY_BLOCK, dtype=jnp.int32)
        strict = (key_pos[None, :] < query_pos[:, None])[None]
        log_keep = jnp.where(strict, jax.nn.log_sigmoid(-scores), 0.0)
        suffix = lax.cumsum(log_keep, axis=2, reverse=True) - log_keep + logsum[:, :, None]
        weight = jnp.where(strict, jnp.exp(jax.nn.log_sigmoid(scores) + suffix), 0.0).astype(
            jnp.bfloat16
        )
        running = running + jnp.einsum(
            "hts,shd->htd", weight, value_block, preferred_element_type=jnp.float32
        )
        return (running, logsum + jnp.sum(log_keep, axis=2))

    initial = (
        jnp.zeros((head_count, row_count, head_depth), jnp.float32),
        jnp.zeros((head_count, row_count), jnp.float32),
    )
    running, logsum = lax.fori_loop(0, last_block + 1, sweep_block, initial)
    return (
        jnp.transpose(running, (1, 0, 2))
        .reshape(row_count, head_count * head_depth)
        .astype(jnp.bfloat16)
    )


def slot_numbers(pair_ids, expert_count):
    one_hot = (pair_ids[..., None] == jnp.arange(expert_count, dtype=jnp.int32)).astype(jnp.int32)
    earlier = jnp.cumsum(one_hot, axis=1) - one_hot
    return jnp.sum(one_hot * earlier, axis=2)


def pack_rows(source_rows, destination, slot_count):
    pair_count = destination.shape[0]
    matches = destination[None, :] == jnp.arange(slot_count, dtype=jnp.int32)[:, None]
    source_index = jnp.sum(
        jnp.where(matches, jnp.arange(pair_count, dtype=jnp.int32)[None, :] // 2, 0), axis=1
    )
    filled = jnp.any(matches, axis=1)
    picked = jnp.take(source_rows, source_index, axis=0)
    return jnp.where(filled[:, None], picked, jnp.zeros_like(picked))


def expand(expert_rows, gate_part, up_part):
    gate_proj = jnp.einsum(
        "rcd,df->rcf", expert_rows, gate_part, preferred_element_type=jnp.float32
    )
    up_proj = jnp.einsum("rcd,df->rcf", expert_rows, up_part, preferred_element_type=jnp.float32)
    return (jax.nn.silu(gate_proj) * up_proj).astype(jnp.bfloat16)


def shards(
    queries,
    key_rows,
    value_rows,
    key_shift,
    out_weight,
    routed_rows,
    expert_ids,
    route_weights,
    gate_weight,
    up_weight,
    down_weight,
):
    tp_count = lax.axis_size("tp")
    local_rows = queries.shape[0]
    heads_here = key_shift.shape[1]
    key_all, value_all, shift_all = sent_together((key_rows, value_rows, key_shift), "ep", 0, 1)
    first_pos = lax.axis_index("ep") * local_rows
    attended = stick_attend(
        queries.reshape(local_rows, heads_here, HEAD), key_all, value_all, shift_all, first_pos
    )
    mixed_rows = sent_and_summed(
        jnp.dot(attended, out_weight, preferred_element_type=jnp.float32).astype(jnp.bfloat16),
        "tp",
        0,
    ).astype(jnp.bfloat16)
    expert_count = lax.axis_size("ep")
    sub_rows = local_rows // tp_count
    capacity = 4 * sub_rows // expert_count
    model_width = routed_rows.shape[1]
    column = lax.axis_index("tp")
    own_ids = lax.dynamic_slice_in_dim(expert_ids, column * sub_rows, sub_rows, 0).reshape(
        1, sub_rows * 2
    )
    own_slot = slot_numbers(own_ids, expert_count)[0]
    own_dest = own_ids[0] * capacity + own_slot
    own_input = lax.dynamic_slice_in_dim(routed_rows, column * sub_rows, sub_rows, 0)
    outgoing = pack_rows(own_input, own_dest, expert_count * capacity).reshape(
        expert_count, capacity, model_width
    )
    arrived = lax.all_to_all(outgoing, "ep", split_axis=0, concat_axis=0, tiled=True)
    hidden = expand(lax.all_gather(arrived, "tp", axis=1, tiled=True), gate_weight[0], up_weight[0])
    unit_count = hidden.shape[2]
    ordered = jnp.transpose(
        hidden.reshape(expert_count, tp_count, capacity, unit_count), (1, 0, 2, 3)
    )
    ordered = ordered.reshape(tp_count * expert_count * capacity, unit_count)
    partial_value = sent_and_summed(
        jnp.dot(ordered, down_weight[0], preferred_element_type=jnp.float32).astype(jnp.bfloat16),
        "tp",
        0,
    ).astype(jnp.bfloat16)
    returned = lax.all_to_all(
        partial_value.reshape(expert_count, capacity, model_width),
        "ep",
        split_axis=0,
        concat_axis=0,
        tiled=True,
    )
    picked = jnp.take(returned.reshape(expert_count * capacity, model_width), own_dest, axis=0)
    picked = picked.reshape(sub_rows, 2, model_width).astype(jnp.float32)
    routed_out = (
        picked[:, 0] * route_weights[:, 0:1] + picked[:, 1] * route_weights[:, 1:2]
    ).astype(jnp.bfloat16)
    return (mixed_rows, routed_out)


def solution(mesh):
    return jax.shard_map(
        shards,
        mesh=mesh,
        in_specs=(
            P("ep", "tp"),
            P("ep", "tp"),
            P("ep", "tp"),
            P("ep", "tp"),
            P("tp", None),
            P("ep", None),
            P("ep", None),
            P(("ep", "tp"), None),
            P("ep", None, "tp"),
            P("ep", None, "tp"),
            P("ep", "tp", None),
        ),
        out_specs=(P(("ep", "tp"), None), P(("ep", "tp"), None)),
        check_vma=False,
    )
```

profile of v0, /device:TPU:228, one launch (start us, length us, event | category | flops | bytes accessed | tf_op | source)
XLA Modules:
  0.0 330.9 jit_solution(5430103602426483478)
XLA Ops:
  11.9 21.6 %all_to_all.20 = bf16[32,2,4096]{2,1,0:T(2,128)(2,1)S(1)} all-to-all(bf16[32,2,4096]{2,1,0:T(2,128)(2,1)S(1)} %broadcast_select_fusion.1), channel_id=1, replica_groups=mesh['ep'=32,'tp'=8] {'ep'}, dimensions={0} | all-to-all | bytes 1048576 | tf_op jit(solution)/shard_map/all_to_all | solution.py:146
  35.8 34.8 %all-gather.5.cloned.1.call-done = bf16[32,16,4096]{2,0,1:T(8,128)(2,1)} async-done(((bf16[32,2,4096]{2,0,1:T(8,128)(2,1)}), bf16[32,16,4096]{2,0,1:T(8,128)(2,1)}) %all-gather.5.cloned.1.call-update) | async-done | bytes 4194320 | tf_op jit(solution)/shard_map/all_gather | solution.py:147
  70.6 3.6 %fusion.21 = f32[32,16,128]{2,0,1:T(8,128)S(1)} fusion(bf16[32,16,4096]{2,0,1:T(8,128)(2,1)} %all-gather.5.cloned.1.call-done, bf16[1,4096,128]{2,1,0:T(8,128)(2,1)S(1)} %copy-done.2), kind=kOutput, calls=%fused_computation.41 | convolution fusion | flops 536870912 | bytes 5505024 | tf_op jit(solution)/shard_map/rcd,df->rcf/dot_general | solution.py:99
  76.9 53.0 %all_to_all.21 = bf16[8,64,4096]{2,1,0:T(8,128)(2,1)} all-to-all(bf16[8,64,4096]{2,1,0:T(8,128)(2,1)S(1)} %bitcast.121), channel_id=1, replica_groups=mesh['ep'=32,'tp'=8] {'tp'}, dimensions={0} | all-to-all | bytes 8388608 | tf_op jit(solution)/shard_map/all_to_all | solution.py:26
  134.1 9.6 %all-to-all-start.3 = ((bf16[32,2,4096]{2,1,0:T(2,128)(2,1)}), bf16[32,2,4096]{2,1,0:T(2,128)(2,1)S(1)}, u32[]{:S(2)}, u32[]{:S(2)}) async-start(bf16[32,2,4096]{2,1,0:T(2,128)(2,1)} %reshape.292), calls=%async_computation.3 | async-start | bytes 1048576 | tf_op jit(solution)/shard_map/all_to_all | solution.py:158
  144.2 19.2 %all-to-all-done.3 = bf16[32,2,4096]{2,1,0:T(2,128)(2,1)S(1)} async-done(((bf16[32,2,4096]{2,1,0:T(2,128)(2,1)}), bf16[32,2,4096]{2,1,0:T(2,128)(2,1)S(1)}, u32[]{:S(2)}, u32[]{:S(2)}) %all-to-all-start.3) | async-done | bytes 524320 | tf_op jit(solution)/shard_map/all_to_all | solution.py:158
  164.5 20.7 %all-gather.3.cloned.1.call-done = bf16[4096,1032]{0,1:T(8,128)(2,1)} async-done(((bf16[128,1032]{0,1:T(8,128)(2,1)}), bf16[4096,1032]{0,1:T(8,128)(2,1)}) %all-gather.3.cloned.1.call-update) | async-done | bytes 8454160 | tf_op jit(solution)/shard_map/all_gather | solution.py:12
  185.3 6.0 %fusion.32 = (bf16[4096,512]{0,1:T(8,128)(2,1)}, bf16[4096,512]{0,1:T(8,128)(2,1)}) fusion(bf16[4096,1032]{0,1:T(8,128)(2,1)} %all-gather.3.cloned.1.call-done), kind=kLoop, calls=%fused_computation.81 | loop fusion | bytes 16777216 | tf_op jit(solution)/shard_map/slice | solution.py:14
  191.3 106.6 %while.13 = (s32[]{:T(128)}, f32[8,128,64]{1,2,0:T(8,128)S(1)}, f32[8,128]{1,0:T(8,128)S(1)}, s32[]{:T(128)}, s32[]{:T(128)}, /*index=5*/bf16[4096,512]{0,1:T(8,...) while((s32[]{:T(128)}, f32[8,128,64]{1,2,0:T(8,128)S(1)}, ...), condition=%wide.region_4.5_spmd.clone, body=%wide.region_0.4_spmd.clone.sunk | while | flops 219303552 | bytes 27235536 | solution.py:73
  195.3 5.1 %fusion.57 = f32[8,128,4,128]{1,0,3,2:T(8,128)S(1)} fusion(f32[8,128,4,128]{1,3,2,0:T(8,128)S(1)} %bitcast.119), kind=kOutput, calls=%fused_computation.21.clone.1 | output fusion | flops 66584576 | bytes 4194304 | tf_op jit(solution)/shard_map/reduce-window
  201.0 3.4 %fusion.59 = bf16[8,128,512]{1,2,0:T(8,128)(2,1)S(1)} fusion(f32[8,128,4,128]{1,3,2,0:T(8,128)S(1)} %copy.90, f32[8,512,128]{2,1,0:T(8,128)S(1)} %get-tuple-element.183, f32[8,128]{1,0:T(8,128)S(1)} %get-tuple-element.201, f32[8,512]{1,0:T(8,128)S(1)} %convert_bitcast_fusion.2, pred[128,512]{0,1:T(8,128)(4,1)S(1)} %broadcast_compare_fusion.2), kind=kLoop, calls=%fused_computation.9.clone.1 | loop fusion | flops 12058624 | bytes 5328896 | tf_op jit(solution)/shard_map/while/body/convert_element_type | solution.py:61
  208.6 5.1 %fusion.57 = f32[8,128,4,128]{1,0,3,2:T(8,128)S(1)} fusion(f32[8,128,4,128]{1,3,2,0:T(8,128)S(1)} %bitcast.119), kind=kOutput, calls=%fused_computation.21.clone.1 | output fusion | flops 66584576 | bytes 4194304 | tf_op jit(solution)/shard_map/reduce-window
  214.3 3.4 %fusion.59 = bf16[8,128,512]{1,2,0:T(8,128)(2,1)S(1)} fusion(f32[8,128,4,128]{1,3,2,0:T(8,128)S(1)} %copy.90, f32[8,512,128]{2,1,0:T(8,128)S(1)} %get-tuple-element.183, f32[8,128]{1,0:T(8,128)S(1)} %get-tuple-element.201, f32[8,512]{1,0:T(8,128)S(1)} %convert_bitcast_fusion.2, pred[128,512]{0,1:T(8,128)(4,1)S(1)} %broadcast_compare_fusion.2), kind=kLoop, calls=%fused_computation.9.clone.1 | loop fusion | flops 12058624 | bytes 5328896 | tf_op jit(solution)/shard_map/while/body/convert_element_type | solution.py:61
  222.0 5.1 %fusion.57 = f32[8,128,4,128]{1,0,3,2:T(8,128)S(1)} fusion(f32[8,128,4,128]{1,3,2,0:T(8,128)S(1)} %bitcast.119), kind=kOutput, calls=%fused_computation.21.clone.1 | output fusion | flops 66584576 | bytes 4194304 | tf_op jit(solution)/shard_map/reduce-window
  227.6 3.4 %fusion.59 = bf16[8,128,512]{1,2,0:T(8,128)(2,1)S(1)} fusion(f32[8,128,4,128]{1,3,2,0:T(8,128)S(1)} %copy.90, f32[8,512,128]{2,1,0:T(8,128)S(1)} %get-tuple-element.183, f32[8,128]{1,0:T(8,128)S(1)} %get-tuple-element.201, f32[8,512]{1,0:T(8,128)S(1)} %convert_bitcast_fusion.2, pred[128,512]{0,1:T(8,128)(4,1)S(1)} %broadcast_compare_fusion.2), kind=kLoop, calls=%fused_computation.9.clone.1 | loop fusion | flops 12058624 | bytes 5328896 | tf_op jit(solution)/shard_map/while/body/convert_element_type | solution.py:61
  235.3 5.1 %fusion.57 = f32[8,128,4,128]{1,0,3,2:T(8,128)S(1)} fusion(f32[8,128,4,128]{1,3,2,0:T(8,128)S(1)} %bitcast.119), kind=kOutput, calls=%fused_computation.21.clone.1 | output fusion | flops 66584576 | bytes 4194304 | tf_op jit(solution)/shard_map/reduce-window
  240.9 3.4 %fusion.59 = bf16[8,128,512]{1,2,0:T(8,128)(2,1)S(1)} fusion(f32[8,128,4,128]{1,3,2,0:T(8,128)S(1)} %copy.90, f32[8,512,128]{2,1,0:T(8,128)S(1)} %get-tuple-element.183, f32[8,128]{1,0:T(8,128)S(1)} %get-tuple-element.201, f32[8,512]{1,0:T(8,128)S(1)} %convert_bitcast_fusion.2, pred[128,512]{0,1:T(8,128)(4,1)S(1)} %broadcast_compare_fusion.2), kind=kLoop, calls=%fused_computation.9.clone.1 | loop fusion | flops 12058624 | bytes 5328896 | tf_op jit(solution)/shard_map/while/body/convert_element_type | solution.py:61
  248.6 5.1 %fusion.57 = f32[8,128,4,128]{1,0,3,2:T(8,128)S(1)} fusion(f32[8,128,4,128]{1,3,2,0:T(8,128)S(1)} %bitcast.119), kind=kOutput, calls=%fused_computation.21.clone.1 | output fusion | flops 66584576 | bytes 4194304 | tf_op jit(solution)/shard_map/reduce-window
  261.9 5.1 %fusion.57 = f32[8,128,4,128]{1,0,3,2:T(8,128)S(1)} fusion(f32[8,128,4,128]{1,3,2,0:T(8,128)S(1)} %bitcast.119), kind=kOutput, calls=%fused_computation.21.clone.1 | output fusion | flops 66584576 | bytes 4194304 | tf_op jit(solution)/shard_map/reduce-window
  275.2 5.1 %fusion.57 = f32[8,128,4,128]{1,0,3,2:T(8,128)S(1)} fusion(f32[8,128,4,128]{1,3,2,0:T(8,128)S(1)} %bitcast.119), kind=kOutput, calls=%fused_computation.21.clone.1 | output fusion | flops 66584576 | bytes 4194304 | tf_op jit(solution)/shard_map/reduce-window
  288.5 5.1 %fusion.57 = f32[8,128,4,128]{1,0,3,2:T(8,128)S(1)} fusion(f32[8,128,4,128]{1,3,2,0:T(8,128)S(1)} %bitcast.119), kind=kOutput, calls=%fused_computation.21.clone.1 | output fusion | flops 66584576 | bytes 4194304 | tf_op jit(solution)/shard_map/reduce-window
  297.9 3.9 %convolution_convert_fusion.1 = bf16[128,4096]{1,0:T(8,128)(2,1)} fusion(bf16[128,512]{0,1:T(8,128)(2,1)S(1)} %bitcast.124, bf16[512,4096]{1,0:T(8,128)(2,1)} %param.17), kind=kOutput, calls=%fused_computation.36 | convolution fusion | flops 537395200 | bytes 5373952 | tf_op jit(solution)/shard_map/dot_general | solution.py:128
  301.9 5.4 %all-to-all-start = ((bf16[8,16,4096]{2,1,0:T(8,128)(2,1)}), bf16[8,16,4096]{2,1,0:T(8,128)(2,1)S(1)}, u32[]{:S(2)}, u32[]{:S(2)}) async-start(bf16[8,16,4096]{2,1,0:T(8,128)(2,1)} %bitcast.3), calls=%async_computation | async-start | bytes 2097152 | tf_op jit(solution)/shard_map/all_to_all | solution.py:26
  308.4 14.9 %all-to-all-done = bf16[8,16,4096]{2,1,0:T(8,128)(2,1)S(1)} async-done(((bf16[8,16,4096]{2,1,0:T(8,128)(2,1)}), bf16[8,16,4096]{2,1,0:T(8,128)(2,1)S(1)}, u32[]{:S(2)}, u32[]{:S(2)}) %all-to-all-start) | async-done | bytes 1048608 | tf_op jit(solution)/shard_map/all_to_all | solution.py:26
  (169 shorter events, 68.5 us)
Async XLA Ops:
  7.2 68.5 %copy-start = (bf16[1,128,4096]{2,1,0:T(8,128)(2,1)S(1)}, bf16[1,128,4096]{2,1,0:T(8,128)(2,1)}, u32[]{:S(2)}) copy-start(bf16[1,128,4096]{2,1,0:T(8,128)(2,1)} %param.23) | copy-start | bytes 3145732
  7.2 63.4 %all-gather.5.cloned.1.call-start = ((), (), s32[]{:S(2)}) async-start(), calls=%async_computation.5 | async-start | bytes 4718592 | tf_op jit(solution)/shard_map/all_gather | solution.py:147
  11.0 23.7 %copy-start.3 = (bf16[128,512]{1,0:T(8,128)(2,1)S(1)}, bf16[128,512]{1,0:T(8,128)(2,1)}, u32[]{:S(2)}) copy-start(bf16[128,512]{1,0:T(8,128)(2,1)} %param.14) | copy-start | bytes 393220
  11.0 23.9 %copy-start.4 = (bf16[128,512]{1,0:T(8,128)(2,1)S(1)}, bf16[128,512]{1,0:T(8,128)(2,1)}, u32[]{:S(2)}) copy-start(bf16[128,512]{1,0:T(8,128)(2,1)} %param.15) | copy-start | bytes 393220
  11.2 23.9 %copy-start.6 = (bf16[128,8]{0,1:T(8,128)(2,1)S(1)}, bf16[128,8]{0,1:T(8,128)(2,1)}, u32[]{:S(2)}) copy-start(bf16[128,8]{0,1:T(8,128)(2,1)} %param.16) | copy-start | bytes 6148
  11.9 58.6 %copy-start.2 = (bf16[1,4096,128]{2,1,0:T(8,128)(2,1)S(1)}, bf16[1,4096,128]{2,1,0:T(8,128)(2,1)}, u32[]{:S(2)}) copy-start(bf16[1,4096,128]{2,1,0:T(8,128)(2,1)} %param.21) | copy-start | bytes 3145732
  34.7 150.6 %all-gather.3.cloned.1.call-start = ((), (), s32[]{:S(2)}) async-start(), calls=%async_computation.4 | async-start | bytes 8718336 | tf_op jit(solution)/shard_map/all_gather | solution.py:12
  70.6 3.6 %copy-start.1 = (bf16[32,16,4096]{2,0,1:T(8,128)(2,1)S(1)}, bf16[32,16,4096]{2,0,1:T(8,128)(2,1)}, u32[]{:S(2)}) copy-start(bf16[32,16,4096]{2,0,1:T(8,128)(2,1)} %all-gather.5.cloned.1.call-done) | copy-start | bytes 12582916
  70.6 3.7 %copy-start.8 = (bf16[1,4096,128]{2,1,0:T(8,128)(2,1)S(1)}, bf16[1,4096,128]{2,1,0:T(8,128)(2,1)}, u32[]{:S(2)}) copy-start(bf16[1,4096,128]{2,1,0:T(8,128)(2,1)} %param.22) | copy-start | bytes 3145732
  132.9 11.1 %copy-start.5 = (bf16[128,512]{1,0:T(8,128)(2,1)S(1)}, bf16[128,512]{1,0:T(8,128)(2,1)}, u32[]{:S(2)}) copy-start(bf16[128,512]{1,0:T(8,128)(2,1)} %param.13) | copy-start | bytes 393220
  132.9 11.3 %copy-start.7 = (f32[16,2]{0,1:T(2,128)S(1)}, f32[16,2]{0,1:T(2,128)}, u32[]{:S(2)}) copy-start(f32[16,2]{0,1:T(2,128)} %param.20) | copy-start | bytes 388
  134.1 29.4 %all-to-all-start.3 = ((bf16[32,2,4096]{2,1,0:T(2,128)(2,1)}), bf16[32,2,4096]{2,1,0:T(2,128)(2,1)S(1)}, u32[]{:S(2)}, u32[]{:S(2)}) async-start(bf16[32,2,4096]{2,1,0:T(2,128)(2,1)} %reshape.292), calls=%async_computation.3 | async-start | bytes 1048576 | tf_op jit(solution)/shard_map/all_to_all | solution.py:158
  185.3 6.0 %slice-start = ((bf16[4096,1032]{0,1:T(8,128)(2,1)}), bf16[4096,8]{0,1:T(8,128)(2,1)S(1)}, s32[]{:S(2)}) async-start(bf16[4096,1032]{0,1:T(8,128)(2,1)} %all-gather.3.cloned.1.call-done), calls=%async_computation.6 | async-start | bytes 131072 | tf_op jit(solution)/shard_map/slice | solution.py:14
  301.9 21.4 %all-to-all-start = ((bf16[8,16,4096]{2,1,0:T(8,128)(2,1)}), bf16[8,16,4096]{2,1,0:T(8,128)(2,1)S(1)}, u32[]{:S(2)}, u32[]{:S(2)}) async-start(bf16[8,16,4096]{2,1,0:T(8,128)(2,1)} %bitcast.3), calls=%async_computation | async-start | bytes 2097152 | tf_op jit(solution)/shard_map/all_to_all | solution.py:26
Sparse Core Ops, SparseCore 0:
  34.8 35.6 all-gather.4
  73.0 112.2 all-gather.2
where the time goes:
time: 331 us
  waiting for transfers between devices  89.6 us (27%)
  other arithmetic  77.9 us (24%)
  blocking collectives  74.6 us (23%)
  matrix products  31.7 us (10%)
  local copies, waits for them, and re-layouts  26.4 us (8%)
  starting transfers between devices  15.1 us (5%)
  between operations  14.4 us (4%)
    all_to_all x1, blocking collectives, sent_and_summed(): lax.all_to_all(tiles, axis, split_axis=0, concat_axis=0, tiled=True)  53 us
    another operation x16, other arithmetic  40.5 us
    all_gather x1, waiting for transfers between devices, shards(): lax.all_gather(arrived, 'tp', axis=1, tiled=True)  34.8 us
    convert_element_type x8, other arithmetic, sweep_block(): jnp.where(strict, jnp.exp(jax.nn.log_sigmoid(scores) + suffix), 0.0)  27.2 us
    all_to_all x1, blocking collectives, shards(): lax.all_to_all(outgoing, 'ep', split_axis=0, concat_axis=0, tiled=True)  21.6 us
    all_gather x1, waiting for transfers between devices, sent_together(): lax.all_gather(both, axis, axis=dim, tiled=True)  20.7 us
    all_to_all x1, waiting for transfers between devices, shards(): lax.all_to_all(partial_value.reshape(expert_count, capacity, model_width)...  19.2 us
    dot_general x8, matrix products, sweep_block(): jnp.einsum('thd,shd->hts', query_rows, key_tile_block, preferred_element_...  19 us
  transfers between devices with their start and end apart: 4, of which 4 were waited for; matrix products, arithmetic and copies ran while one was open for 4% of the time, Pallas kernels for 0%

commit v1 on v0

--- a/solution.py
+++ b/solution.py
@@ -1,3 +1,4 @@
+import functools
 import jax
 import jax.numpy as jnp
 from jax import lax
@@ -5,6 +6,15 @@
 
 HEAD = 64
 KEY_BLOCK = 512
+
+
+def cut_rounds(x_in, net_axis):
+    sides = lax.axis_size(net_axis)
+    rack = tuple((sides if s == 1 else 1 for s in range(x_in.ndim)))
+    return lax.all_to_all(jnp.tile(x_in, rack), net_axis, split_axis=1, concat_axis=1, tiled=True)
+
+
+show_local_data = functools.partial(cut_rounds, net_axis="tp")
 
 
 def sent_together(arrays, axis, dim, along):
@@ -144,7 +154,7 @@
         expert_count, capacity, model_width
     )
     arrived = lax.all_to_all(outgoing, "ep", split_axis=0, concat_axis=0, tiled=True)
-    hidden = expand(lax.all_gather(arrived, "tp", axis=1, tiled=True), gate_weight[0], up_weight[0])
+    hidden = expand(show_local_data(arrived), gate_weight[0], up_weight[0])
     unit_count = hidden.shape[2]
     ordered = jnp.transpose(
         hidden.reshape(expert_count, tp_count, capacity, unit_count), (1, 0, 2, 3)

time: 331 us -> 326 us (0.985)
  waiting for transfers between devices: 89.6 us -> 27.1 us
  blocking collectives: 74.6 us -> 131 us
    all_to_all x0 -> x1, blocking collectives: none -> 54.1 us  [cut_rounds(): lax.all_to_all(jnp.tile(x_in, rack), net_axis, split_axis=1, concat_axis=...]
    all_gather x1 -> x0, waiting for transfers between devices: 34.8 us -> none  [shards(): lax.all_gather(arrived, 'tp', axis=1, tiled=True)]
    all_gather x1, waiting for transfers between devices: 20.7 us -> 0.02 us  [sent_together(): lax.all_gather(both, axis, axis=dim, tiled=True)]
    all_to_all x1, waiting for transfers between devices: 19.2 us -> 12.3 us  [shards(): lax.all_to_all(partial_value.reshape(expert_count, capacity, model_width)...]
  transfers between devices with their start and end apart: 4 -> 3, of which waited for: 4 -> 2; matrix products, arithmetic and copies ran while one was open for 4% -> 5% of each run, Pallas kernels for 0% -> 0%
where the time goes in v1:
time: 326 us; the launch traced here: 323 us
  blocking collectives  131 us (40%)
  other arithmetic  78.5 us (24%)
  matrix products  29.4 us (9%)
  local copies, waits for them, and re-layouts  27.8 us (9%)
  waiting for transfers between devices  27.1 us (8%)
  between operations  14.4 us (4%)
  starting transfers between devices  13.4 us (4%)
    all_to_all x1, blocking collectives, cut_rounds(): lax.all_to_all(jnp.tile(x_in, rack), net_axis, split_axis=1, concat_axis=...  54.1 us
    all_to_all x1, blocking collectives, sent_and_summed(): lax.all_to_all(tiles, axis, split_axis=0, concat_axis=0, tiled=True)  53 us
    another operation x16, other arithmetic  40.5 us
    convert_element_type x8, other arithmetic, sweep_block(): jnp.where(strict, jnp.exp(jax.nn.log_sigmoid(scores) + suffix), 0.0)  27.2 us
    all_to_all x1, blocking collectives, shards(): lax.all_to_all(outgoing, 'ep', split_axis=0, concat_axis=0, tiled=True)  24.2 us
    dot_general x8, matrix products, sweep_block(): jnp.einsum('thd,shd->hts', query_rows, key_tile_block, preferred_element_...  19 us
    all_to_all x1, waiting for transfers between devices, sent_and_summed(): lax.all_to_all(tiles, axis, split_axis=0, concat_axis=0, tiled=True)  14.8 us
    all_to_all x1, waiting for transfers between devices, shards(): lax.all_to_all(partial_value.reshape(expert_count, capacity, model_width)...  12.3 us
  transfers between devices with their start and end apart: 3, of which 2 were waited for; matrix products, arithmetic and copies ran while one was open for 5% of the time, Pallas kernels for 0%

profile of v1, /device:TPU:228, one launch (start us, length us, event | category | flops | bytes accessed | tf_op | source)
XLA Modules:
  0.0 323.0 jit_solution(10118431513816423314)
XLA Ops:
  15.4 24.2 %all_to_all.25 = bf16[32,2,4096]{2,1,0:T(2,128)(2,1)S(1)} all-to-all(bf16[32,2,4096]{2,1,0:T(2,128)(2,1)S(1)} %broadcast_select_fusion.1), channel_id=1, replica_groups=mesh['ep'=32,'tp'=8] {'ep'}, dimensions={0} | all-to-all | bytes 1048576 | tf_op jit(solution)/shard_map/all_to_all | solution.py:156
  40.4 54.1 %all_to_all.26 = bf16[32,16,4096]{2,0,1:T(8,128)(2,1)S(1)} all-to-all(bf16[32,16,4096]{2,0,1:T(8,128)(2,1)S(1)} %bitcast.123), channel_id=1, replica_groups=mesh['ep'=32,'tp'=8] {'tp'}, dimensions={1} | all-to-all | bytes 8388608 | tf_op jit(solution)/shard_map/all_to_all | solution.py:14
  98.5 53.0 %all_to_all.27 = bf16[8,64,4096]{2,1,0:T(8,128)(2,1)} all-to-all(bf16[8,64,4096]{2,1,0:T(8,128)(2,1)S(1)} %bitcast.122), channel_id=1, replica_groups=mesh['ep'=32,'tp'=8] {'tp'}, dimensions={0} | all-to-all | bytes 8388608 | tf_op jit(solution)/shard_map/all_to_all | solution.py:36
  155.6 9.8 %all-to-all-start.4 = ((bf16[32,2,4096]{2,1,0:T(2,128)(2,1)}), bf16[32,2,4096]{2,1,0:T(2,128)(2,1)S(1)}, u32[]{:S(2)}, u32[]{:S(2)}) async-start(bf16[32,2,4096]{2,1,0:T(2,128)(2,1)} %reshape.296), calls=%async_computation.4 | async-start | bytes 1048576 | tf_op jit(solution)/shard_map/all_to_all | solution.py:168
  165.9 12.3 %all-to-all-done.4 = bf16[32,2,4096]{2,1,0:T(2,128)(2,1)S(1)} async-done(((bf16[32,2,4096]{2,1,0:T(2,128)(2,1)}), bf16[32,2,4096]{2,1,0:T(2,128)(2,1)S(1)}, u32[]{:S(2)}, u32[]{:S(2)}) %all-to-all-start.4) | async-done | bytes 524320 | tf_op jit(solution)/shard_map/all_to_all | solution.py:168
  179.3 6.0 %fusion.32 = (bf16[4096,512]{0,1:T(8,128)(2,1)}, bf16[4096,512]{0,1:T(8,128)(2,1)}) fusion(bf16[4096,1032]{0,1:T(8,128)(2,1)} %all-gather.2.cloned.1.call-done), kind=kLoop, calls=%fused_computation.81 | loop fusion | bytes 16777216 | tf_op jit(solution)/shard_map/slice | solution.py:24
  185.3 106.6 %while.13 = (s32[]{:T(128)}, f32[8,128,64]{1,2,0:T(8,128)S(1)}, f32[8,128]{1,0:T(8,128)S(1)}, s32[]{:T(128)}, s32[]{:T(128)}, /*index=5*/bf16[4096,512]{0,1:T(8,...) while((s32[]{:T(128)}, f32[8,128,64]{1,2,0:T(8,128)S(1)}, ...), condition=%wide.region_4.5_spmd.clone, body=%wide.region_0.4_spmd.clone.sunk | while | flops 219303552 | bytes 27235536 | solution.py:83
  189.4 5.1 %fusion.57 = f32[8,128,4,128]{1,0,3,2:T(8,128)S(1)} fusion(f32[8,128,4,128]{1,3,2,0:T(8,128)S(1)} %bitcast.120), kind=kOutput, calls=%fused_computation.21.clone.1 | output fusion | flops 66584576 | bytes 4194304 | tf_op jit(solution)/shard_map/reduce-window
  195.1 3.4 %fusion.59 = bf16[8,128,512]{1,2,0:T(8,128)(2,1)S(1)} fusion(f32[8,128,4,128]{1,3,2,0:T(8,128)S(1)} %copy.77, f32[8,512,128]{2,1,0:T(8,128)S(1)} %get-tuple-element.183, f32[8,128]{1,0:T(8,128)S(1)} %get-tuple-element.201, f32[8,512]{1,0:T(8,128)S(1)} %convert_bitcast_fusion.2, pred[128,512]{0,1:T(8,128)(4,1)S(1)} %broadcast_compare_fusion.2), kind=kLoop, calls=%fused_computation.9.clone.1 | loop fusion | flops 12058624 | bytes 5328896 | tf_op jit(solution)/shard_map/while/body/convert_element_type | solution.py:71
  202.7 5.1 %fusion.57 = f32[8,128,4,128]{1,0,3,2:T(8,128)S(1)} fusion(f32[8,128,4,128]{1,3,2,0:T(8,128)S(1)} %bitcast.120), kind=kOutput, calls=%fused_computation.21.clone.1 | output fusion | flops 66584576 | bytes 4194304 | tf_op jit(solution)/shard_map/reduce-window
  216.0 5.1 %fusion.57 = f32[8,128,4,128]{1,0,3,2:T(8,128)S(1)} fusion(f32[8,128,4,128]{1,3,2,0:T(8,128)S(1)} %bitcast.120), kind=kOutput, calls=%fused_computation.21.clone.1 | output fusion | flops 66584576 | bytes 4194304 | tf_op jit(solution)/shard_map/reduce-window
  221.7 3.4 %fusion.59 = bf16[8,128,512]{1,2,0:T(8,128)(2,1)S(1)} fusion(f32[8,128,4,128]{1,3,2,0:T(8,128)S(1)} %copy.77, f32[8,512,128]{2,1,0:T(8,128)S(1)} %get-tuple-element.183, f32[8,128]{1,0:T(8,128)S(1)} %get-tuple-element.201, f32[8,512]{1,0:T(8,128)S(1)} %convert_bitcast_fusion.2, pred[128,512]{0,1:T(8,128)(4,1)S(1)} %broadcast_compare_fusion.2), kind=kLoop, calls=%fused_computation.9.clone.1 | loop fusion | flops 12058624 | bytes 5328896 | tf_op jit(solution)/shard_map/while/body/convert_element_type | solution.py:71
  229.3 5.1 %fusion.57 = f32[8,128,4,128]{1,0,3,2:T(8,128)S(1)} fusion(f32[8,128,4,128]{1,3,2,0:T(8,128)S(1)} %bitcast.120), kind=kOutput, calls=%fused_computation.21.clone.1 | output fusion | flops 66584576 | bytes 4194304 | tf_op jit(solution)/shard_map/reduce-window
  235.0 3.4 %fusion.59 = bf16[8,128,512]{1,2,0:T(8,128)(2,1)S(1)} fusion(f32[8,128,4,128]{1,3,2,0:T(8,128)S(1)} %copy.77, f32[8,512,128]{2,1,0:T(8,128)S(1)} %get-tuple-element.183, f32[8,128]{1,0:T(8,128)S(1)} %get-tuple-element.201, f32[8,512]{1,0:T(8,128)S(1)} %convert_bitcast_fusion.2, pred[128,512]{0,1:T(8,128)(4,1)S(1)} %broadcast_compare_fusion.2), kind=kLoop, calls=%fused_computation.9.clone.1 | loop fusion | flops 12058624 | bytes 5328896 | tf_op jit(solution)/shard_map/while/body/convert_element_type | solution.py:71
  242.6 5.1 %fusion.57 = f32[8,128,4,128]{1,0,3,2:T(8,128)S(1)} fusion(f32[8,128,4,128]{1,3,2,0:T(8,128)S(1)} %bitcast.120), kind=kOutput, calls=%fused_computation.21.clone.1 | output fusion | flops 66584576 | bytes 4194304 | tf_op jit(solution)/shard_map/reduce-window
  248.3 3.4 %fusion.59 = bf16[8,128,512]{1,2,0:T(8,128)(2,1)S(1)} fusion(f32[8,128,4,128]{1,3,2,0:T(8,128)S(1)} %copy.77, f32[8,512,128]{2,1,0:T(8,128)S(1)} %get-tuple-element.183, f32[8,128]{1,0:T(8,128)S(1)} %get-tuple-element.201, f32[8,512]{1,0:T(8,128)S(1)} %convert_bitcast_fusion.2, pred[128,512]{0,1:T(8,128)(4,1)S(1)} %broadcast_compare_fusion.2), kind=kLoop, calls=%fused_computation.9.clone.1 | loop fusion | flops 12058624 | bytes 5328896 | tf_op jit(solution)/shard_map/while/body/convert_element_type | solution.py:71
  255.9 5.1 %fusion.57 = f32[8,128,4,128]{1,0,3,2:T(8,128)S(1)} fusion(f32[8,128,4,128]{1,3,2,0:T(8,128)S(1)} %bitcast.120), kind=kOutput, calls=%fused_computation.21.clone.1 | output fusion | flops 66584576 | bytes 4194304 | tf_op jit(solution)/shard_map/reduce-window
  261.6 3.4 %fusion.59 = bf16[8,128,512]{1,2,0:T(8,128)(2,1)S(1)} fusion(f32[8,128,4,128]{1,3,2,0:T(8,128)S(1)} %copy.77, f32[8,512,128]{2,1,0:T(8,128)S(1)} %get-tuple-element.183, f32[8,128]{1,0:T(8,128)S(1)} %get-tuple-element.201, f32[8,512]{1,0:T(8,128)S(1)} %convert_bitcast_fusion.2, pred[128,512]{0,1:T(8,128)(4,1)S(1)} %broadcast_compare_fusion.2), kind=kLoop, calls=%fused_computation.9.clone.1 | loop fusion | flops 12058624 | bytes 5328896 | tf_op jit(solution)/shard_map/while/body/convert_element_type | solution.py:71
  269.2 5.1 %fusion.57 = f32[8,128,4,128]{1,0,3,2:T(8,128)S(1)} fusion(f32[8,128,4,128]{1,3,2,0:T(8,128)S(1)} %bitcast.120), kind=kOutput, calls=%fused_computation.21.clone.1 | output fusion | flops 66584576 | bytes 4194304 | tf_op jit(solution)/shard_map/reduce-window
  274.9 3.4 %fusion.59 = bf16[8,128,512]{1,2,0:T(8,128)(2,1)S(1)} fusion(f32[8,128,4,128]{1,3,2,0:T(8,128)S(1)} %copy.77, f32[8,512,128]{2,1,0:T(8,128)S(1)} %get-tuple-element.183, f32[8,128]{1,0:T(8,128)S(1)} %get-tuple-element.201, f32[8,512]{1,0:T(8,128)S(1)} %convert_bitcast_fusion.2, pred[128,512]{0,1:T(8,128)(4,1)S(1)} %broadcast_compare_fusion.2), kind=kLoop, calls=%fused_computation.9.clone.1 | loop fusion | flops 12058624 | bytes 5328896 | tf_op jit(solution)/shard_map/while/body/convert_element_type | solution.py:71
  282.5 5.1 %fusion.57 = f32[8,128,4,128]{1,0,3,2:T(8,128)S(1)} fusion(f32[8,128,4,128]{1,3,2,0:T(8,128)S(1)} %bitcast.120), kind=kOutput, calls=%fused_computation.21.clone.1 | output fusion | flops 66584576 | bytes 4194304 | tf_op jit(solution)/shard_map/reduce-window
  292.0 3.9 %convolution_convert_fusion.1 = bf16[128,4096]{1,0:T(8,128)(2,1)} fusion(bf16[128,512]{0,1:T(8,128)(2,1)S(1)} %bitcast.126, bf16[512,4096]{1,0:T(8,128)(2,1)} %param.17), kind=kOutput, calls=%fused_computation.36 | convolution fusion | flops 537395200 | bytes 5373952 | tf_op jit(solution)/shard_map/dot_general | solution.py:138
  295.9 3.6 %all-to-all-start = ((bf16[8,16,4096]{2,1,0:T(8,128)(2,1)}), bf16[8,16,4096]{2,1,0:T(8,128)(2,1)S(1)}, u32[]{:S(2)}, u32[]{:S(2)}) async-start(bf16[8,16,4096]{2,1,0:T(8,128)(2,1)} %bitcast.3), calls=%async_computation | async-start | bytes 2097152 | tf_op jit(solution)/shard_map/all_to_all | solution.py:36
  300.6 14.8 %all-to-all-done = bf16[8,16,4096]{2,1,0:T(8,128)(2,1)S(1)} async-done(((bf16[8,16,4096]{2,1,0:T(8,128)(2,1)}), bf16[8,16,4096]{2,1,0:T(8,128)(2,1)S(1)}, u32[]{:S(2)}, u32[]{:S(2)}) %all-to-all-start) | async-done | bytes 1048608 | tf_op jit(solution)/shard_map/all_to_all | solution.py:36
  (160 shorter events, 65.0 us)
Async XLA Ops:
  7.2 90.0 %copy-start = (bf16[1,128,4096]{2,1,0:T(8,128)(2,1)S(1)}, bf16[1,128,4096]{2,1,0:T(8,128)(2,1)}, u32[]{:S(2)}) copy-start(bf16[1,128,4096]{2,1,0:T(8,128)(2,1)} %param.23) | copy-start | bytes 3145732
  7.2 172.1 %all-gather.2.cloned.1.call-start = ((), (), s32[]{:S(2)}) async-start(), calls=%async_computation.5 | async-start | bytes 8718336 | tf_op jit(solution)/shard_map/all_gather | solution.py:22
  40.4 54.1 %copy-start.1 = (bf16[1,4096,128]{2,1,0:T(8,128)(2,1)S(1)}, bf16[1,4096,128]{2,1,0:T(8,128)(2,1)}, u32[]{:S(2)}) copy-start(bf16[1,4096,128]{2,1,0:T(8,128)(2,1)} %param.21) | copy-start | bytes 3145732
  94.6 1.3 copy-start.4
  154.4 11.3 %copy-start.2 = (bf16[128,512]{1,0:T(8,128)(2,1)S(1)}, bf16[128,512]{1,0:T(8,128)(2,1)}, u32[]{:S(2)}) copy-start(bf16[128,512]{1,0:T(8,128)(2,1)} %param.13) | copy-start | bytes 393220
  154.4 11.5 %copy-start.3 = (f32[16,2]{0,1:T(2,128)S(1)}, f32[16,2]{0,1:T(2,128)}, u32[]{:S(2)}) copy-start(f32[16,2]{0,1:T(2,128)} %param.20) | copy-start | bytes 388
  155.6 22.6 %all-to-all-start.4 = ((bf16[32,2,4096]{2,1,0:T(2,128)(2,1)}), bf16[32,2,4096]{2,1,0:T(2,128)(2,1)S(1)}, u32[]{:S(2)}, u32[]{:S(2)}) async-start(bf16[32,2,4096]{2,1,0:T(2,128)(2,1)} %reshape.296), calls=%async_computation.4 | async-start | bytes 1048576 | tf_op jit(solution)/shard_map/all_to_all | solution.py:168
  179.3 6.0 %slice-start = ((bf16[4096,1032]{0,1:T(8,128)(2,1)}), bf16[4096,8]{0,1:T(8,128)(2,1)S(1)}, s32[]{:S(2)}) async-start(bf16[4096,1032]{0,1:T(8,128)(2,1)} %all-gather.2.cloned.1.call-done), calls=%async_computation.6 | async-start | bytes 131072 | tf_op jit(solution)/shard_map/slice | solution.py:24
  295.9 19.4 %all-to-all-start = ((bf16[8,16,4096]{2,1,0:T(8,128)(2,1)}), bf16[8,16,4096]{2,1,0:T(8,128)(2,1)S(1)}, u32[]{:S(2)}, u32[]{:S(2)}) async-start(bf16[8,16,4096]{2,1,0:T(8,128)(2,1)} %bitcast.3), calls=%async_computation | async-start | bytes 2097152 | tf_op jit(solution)/shard_map/all_to_all | solution.py:36
Sparse Core Ops, SparseCore 0:
  10.9 108.6 all-gather.1
